TPU v7x, 256 devices: a 4x2x16 block of a 4x16x16 slice. The times are simulated.
256 devices in a mesh: grp: 2 (over y), fs: 16 (over z), tp: 8 (over x, core).
Axes of the slice: x: 4, y: 2, z: 16, core: 2. Of those that a mesh axis runs over, the one named last changes fastest.
The devices are a block of a 4x16x16 slice.
Arguments:
- tokens: bfloat16 [32768, 2048], P(('grp', 'fs'), 'tp'), parts along dimension 0, may hold values from -50 to 50
- mix_gain: float32 [2048], replicated, may hold values from 0.1 to 1.9
- value_proj: bfloat16 [2048, 1024], P('fs', 'tp'), may hold values from -0.125 to 0.125
- gate_proj: bfloat16 [2048, 1024], P('fs', 'tp'), may hold values from -0.125 to 0.125
- conv_taps: float32 [31, 1024], P(None, 'tp'), may hold values from -1 to 1
- chan_gain: float32 [1024], replicated, may hold values from 0.1 to 1.9
- chan_shift: float32 [1024], replicated, may hold values from -3 to 3
- mix_out: bfloat16 [1024, 2048], P('fs', 'tp'), may hold values from -0.1875 to 0.1875
- mlp_gain: float32 [2048], replicated, may hold values from 0.1 to 1.9
- mlp_gate: bfloat16 [2048, 5632], P('fs', 'tp'), may hold values from -0.125 to 0.125
- mlp_up: bfloat16 [2048, 5632], P('fs', 'tp'), may hold values from -0.125 to 0.125
- gate_taps: float32 [3, 5632], P(None, 'tp'), may hold values from -3.5 to 3.5
- up_taps: float32 [3, 5632], P(None, 'tp'), may hold values from -3.5 to 3.5
- mlp_down: bfloat16 [5632, 2048], P('tp', 'fs'), may hold values from -0.078125 to 0.078125
- final_gain: float32 [2048], P('tp'), may hold values from 0.1 to 1.9
Outputs:
- layer_out: bfloat16 [32768, 2048], P(('grp', 'fs'), 'tp'), parts along dimension 0
There are 2 independent parts, one for each index of `grp`. A program takes and returns all parts, laid end to end along the dimension named above; an argument that names none is the same for every part. Nothing has to cross between parts.
All inputs are finite; a program needn't handle non-finite values.
Results may differ from a plain program's by a relative error of at most 0.0095.
Values may be sent and summed in bfloat16 or wider, within the bound.
A program may use at most 128 MiB of HBM per device.

v0:
```python
import jax
import jax.numpy as jnp
from jax import lax
from jax.sharding import PartitionSpec as P


def side_by_side(arrays, axis, dim, along):
    ends, at = ([], 0)
    for a in arrays[:-1]:
        at += a.shape[along]
        ends.append(at)
    both = jnp.concatenate(arrays, axis=along)
    return tuple(jnp.split(lax.all_gather(both, axis, axis=dim, tiled=True), ends, axis=along))


def rms_scale(values, gain):
    return values * lax.rsqrt(jnp.mean(values * values, axis=-1, keepdims=True) + 1e-06) * gain


def along_sequence(values, taps):
    width = taps.shape[0]
    half = (width - 1) // 2
    length = values.shape[0]
    padded = jnp.pad(values, ((half, width - 1 - half), (0, 0)))
    total = jnp.zeros_like(values)
    for offset in range(width):
        total = total + taps[offset] * padded[offset : offset + length]
    return total


def local(
    tokens,
    mix_gain,
    value_proj,
    gate_proj,
    conv_taps,
    chan_gain,
    chan_shift,
    mix_out,
    mlp_gain,
    mlp_gate,
    mlp_up,
    gate_taps,
    up_taps,
    mlp_down,
    final_gain,
):
    width_tp = lax.axis_size("tp")
    whole = lax.all_gather(tokens, "tp", axis=1, tiled=True)
    normed = rms_scale(whole.astype(jnp.float32), mix_gain).astype(jnp.bfloat16)
    first = jnp.dot(
        normed,
        lax.all_gather(value_proj, "fs", axis=0, tiled=True),
        preferred_element_type=jnp.float32,
    )
    second = jnp.dot(
        normed,
        lax.all_gather(gate_proj, "fs", axis=0, tiled=True),
        preferred_element_type=jnp.float32,
    )
    glu = first * jax.nn.sigmoid(second)
    conv_out = along_sequence(glu, conv_taps).astype(jnp.bfloat16)
    conv_all = lax.all_gather(conv_out, "tp", axis=1, tiled=True).astype(jnp.float32)
    mean = jnp.mean(conv_all, axis=-1, keepdims=True)
    var = jnp.mean(conv_all * conv_all, axis=-1, keepdims=True) - mean * mean
    chan_norm = (conv_all - mean) * lax.rsqrt(var + 1e-05) * chan_gain + chan_shift
    hidden_mix = jax.nn.silu(chan_norm).astype(jnp.bfloat16)
    mixer_result = jnp.dot(
        hidden_mix,
        lax.all_gather(mix_out, "fs", axis=0, tiled=True),
        preferred_element_type=jnp.float32,
    )
    mixed = (tokens.astype(jnp.float32) + mixer_result).astype(jnp.bfloat16)
    whole_two = lax.all_gather(mixed, "tp", axis=1, tiled=True)
    normed_two = rms_scale(whole_two.astype(jnp.float32), mlp_gain).astype(jnp.bfloat16)
    full_gate, full_up = side_by_side((mlp_gate, mlp_up), "fs", 0, 1)
    gate_pre = jnp.dot(normed_two, full_gate, preferred_element_type=jnp.float32)
    up_pre = jnp.dot(normed_two, full_up, preferred_element_type=jnp.float32)
    gate_conv = along_sequence(gate_pre, gate_taps)
    up_conv = along_sequence(up_pre, up_taps)
    hidden_mlp = (jax.nn.silu(gate_conv) * up_conv).astype(jnp.bfloat16)
    partial_terms = jnp.dot(
        hidden_mlp,
        lax.all_gather(mlp_down, "fs", axis=1, tiled=True),
        preferred_element_type=jnp.float32,
    )
    mlp_out = lax.psum_scatter(
        partial_terms.astype(jnp.bfloat16), "tp", scatter_dimension=1, tiled=True
    ).astype(jnp.float32)
    summed = mixed.astype(jnp.float32) + mlp_out
    squares = lax.psum(jnp.sum(summed * summed, axis=-1, keepdims=True), "tp")
    all_features = summed.shape[1] * width_tp
    layer_out = summed * lax.rsqrt(squares / all_features + 1e-06) * final_gain
    return layer_out.astype(jnp.bfloat16)


def solution(mesh):
    return jax.shard_map(
        local,
        mesh=mesh,
        in_specs=(
            P(("grp", "fs"), "tp"),
            P(),
            P("fs", "tp"),
            P("fs", "tp"),
            P(None, "tp"),
            P(),
            P(),
            P("fs", "tp"),
            P(),
            P("fs", "tp"),
            P("fs", "tp"),
            P(None, "tp"),
            P(None, "tp"),
            P("tp", "fs"),
            P("tp"),
        ),
        out_specs=P(("grp", "fs"), "tp"),
        check_vma=False,
    )
```

profile of v0, /device:TPU:33, one launch (start us, length us, event | category | flops | bytes accessed | tf_op | source)
XLA Modules:
  0.0 436.4 jit_solution(2931170777919696324)
XLA Ops:
  6.6 0.7 all-gather.6.cloned.1.call-update
  7.4 1.0 slice_bitcast_fusion.29
  8.3 1.0 slice_bitcast_fusion.30
  9.4 46.4 %all_gather.26 = bf16[2048,128]{1,0:T(8,128)(2,1)S(1)} all-gather(bf16[128,128]{1,0:T(8,128)(2,1)} %param.18), channel_id=1, replica_groups=mesh['grp'=2,'fs'=16,'tp'=8] {'fs'}, dimensions={0}, use_global_device_ids=true | all-gather | bytes 557056 | tf_op jit(solution)/shard_map/all_gather | solution.py:58
  55.7 23.2 %all_gather.25 = bf16[2048,128]{1,0:T(8,128)(2,1)S(1)} all-gather(bf16[128,128]{1,0:T(8,128)(2,1)} %param.17), channel_id=1, replica_groups=mesh['grp'=2,'fs'=16,'tp'=8] {'fs'}, dimensions={0}, use_global_device_ids=true | all-gather | bytes 557056 | tf_op jit(solution)/shard_map/all_gather | solution.py:53
  79.0 3.2 fusion
  82.2 0.2 copy-done.1
  82.4 1.3 fusion.41
  83.8 1.3 convolution_multiply_fusion
  85.1 2.8 add_convert_fusion
  88.0 0.1 all-gather.10.cloned.1.call-start
  88.1 0.2 copy.19
  88.3 23.6 %all_gather.28 = bf16[1024,256]{1,0:T(8,128)(2,1)S(1)} all-gather(bf16[64,256]{1,0:T(8,128)(2,1)S(1)} %copy-done.6), channel_id=1, replica_groups=mesh['grp'=2,'fs'=16,'tp'=8] {'fs'}, dimensions={0}, use_global_device_ids=true | all-gather | bytes 557056 | tf_op jit(solution)/shard_map/all_gather | solution.py:70
  111.9 16.1 %all-gather.8.cloned.1.call-done = bf16[1024,1024]{1,0:T(8,128)(2,1)} async-done(((bf16[1024,128]{1,0:T(8,128)(2,1)}), bf16[1024,1024]{1,0:T(8,128)(2,1)}) %all-gather.8.cloned.1.call-update) | async-done | bytes 2097168 | tf_op jit(solution)/shard_map/all_gather | solution.py:63
  128.1 2.3 convert_reduce_fusion
  130.4 4.4 %fusion.36 = bf16[1024,256]{0,1:T(8,128)(2,1)} fusion(bf16[1024,256]{1,0:T(8,128)(2,1)S(1)} %all_gather.28, bf16[1024,1024]{1,0:T(8,128)(2,1)} %all-gather.8.cloned.1.call-done, f32[1024]{0:T(1024)S(1)} %copy-done.13, f32[1024]{0:T(1024)S(1)} %copy-done.14, f32[1024]{0:T(1024)S(1)} %get-tuple-element.45, f32[1024]{0:T(1024)S(1)} %get-tuple-element.44, ...), kind=kOutput, calls=%fused_computation.44 | convolution fusion | flops 548143104 | bytes 3686400 | tf_op jit(solution)/shard_map/dot_general | solution.py:68
  134.9 0.1 all-gather.12.cloned.1.call-start
  135.0 0.8 pad_maximum_fusion
  135.9 0.6 all-gather.14.cloned.1.call-update
  136.5 0.2 reduce-scatter.2.cloned.1.call-start
  136.8 36.9 %all-gather.10.cloned.1.call-done = bf16[1024,2048]{0,1:T(8,128)(2,1)} async-done(((bf16[1024,256]{0,1:T(8,128)(2,1)}), bf16[1024,2048]{0,1:T(8,128)(2,1)}) %all-gather.10.cloned.1.call-update) | async-done | bytes 4194320 | tf_op jit(solution)/shard_map/all_gather | solution.py:74
  173.7 3.1 fusion.3
  176.8 93.9 %all-gather.12.cloned.1.call-done = bf16[2048,1408]{0,1:T(8,128)(2,1)} async-done(((bf16[128,1408]{0,1:T(8,128)(2,1)}), bf16[2048,1408]{0,1:T(8,128)(2,1)}) %all-gather.12.cloned.1.call-update) | async-done | bytes 5767184 | tf_op jit(solution)/shard_map/all_gather | solution.py:13
  270.7 6.4 %fusion.28 = f32[1024,704]{0,1:T(8,128)S(1)} fusion(bf16[2048,1408]{0,1:T(8,128)(2,1)} %all-gather.12.cloned.1.call-done, bf16[1024,2048]{0,1:T(8,128)(2,1)} %all-gather.10.cloned.1.call-done, f32[2048]{0:T(1024)S(1)} %copy-done.12, f32[1024]{0:T(1024)S(1)} %add_rsqrt_fusion.1), kind=kOutput, calls=%fused_computation.40 | convolution fusion | flops 2961178624 | bytes 9973760 | tf_op jit(solution)/shard_map/dot_general | solution.py:77
  277.1 4.8 %fusion.26 = f32[1024,704]{0,1:T(8,128)} fusion(bf16[2048,1408]{0,1:T(8,128)(2,1)S(1)} %copy-done.10, bf16[1024,2048]{0,1:T(8,128)(2,1)S(1)} %copy-done.2, f32[2048]{0:T(1024)S(1)} %copy-done.12, f32[1024]{0:T(1024)S(1)} %add_rsqrt_fusion.1), kind=kOutput, calls=%fused_computation.38 | convolution fusion | flops 2961178624 | bytes 9973760 | tf_op jit(solution)/shard_map/dot_general | solution.py:78
  282.0 68.3 %all-gather.14.cloned.1.call-done = bf16[704,2048]{1,0:T(8,128)(2,1)} async-done(((bf16[704,128]{1,0:T(8,128)(2,1)}), bf16[704,2048]{1,0:T(8,128)(2,1)}) %all-gather.14.cloned.1.call-update) | async-done | bytes 2883600 | tf_op jit(solution)/shard_map/all_gather | solution.py:84
  350.3 12.2 %convolution_convert_fusion = bf16[1024,2048]{0,1:T(8,128)(2,1)} fusion(bf16[704,2048]{1,0:T(8,128)(2,1)} %all-gather.14.cloned.1.call-done, f32[1024,704]{0,1:T(8,128)} %fusion.26, f32[1024,704]{0,1:T(8,128)S(1)} %fusion.28, f32[704]{0:T(1024)S(1)} %get-tuple-element.11, f32[704]{0:T(1024)S(1)} %get-tuple-element.12, f32[704]{0:T(1024)S(1)} %get-tuple-element.10, ...), kind=kOutput, calls=%fused_computation.23 | convolution fusion | flops 2966421504 | bytes 12861952 | tf_op jit(solution)/shard_map/dot_general | solution.py:82
  362.5 48.7 %reduce-scatter.2.cloned.1.call-done = bf16[1024,256]{0,1:T(8,128)(2,1)} async-done(((bf16[1024,2048]{0,1:T(8,128)(2,1)}), bf16[1024,256]{0,1:T(8,128)(2,1)}) %reduce-scatter.2.cloned.1.call-update) | async-done | bytes 524304 | tf_op jit(solution)/shard_map/reduce_scatter | solution.py:87
  411.2 1.2 multiply_reduce_fusion
  412.4 14.8 %psum.7 = f32[1024,1]{0,1:T(1,128)S(1)} all-reduce(f32[1024,1]{0,1:T(1,128)S(1)} %bitcast.69), channel_id=1, replica_groups=mesh['grp'=2,'fs'=16,'tp'=8] {'tp'}, use_global_device_ids=true, to_apply=%region_6.7 | all-reduce | flops 1024 | bytes 8192 | tf_op jit(solution)/shard_map/psum | solution.py:91
  427.3 1.2 multiply_convert_fusion
  428.5 1.0 copy.21
  (42 shorter events, 0.5 us)
Async XLA Ops:
  6.5 75.7 %copy-start.11 = (f32[2048]{0:T(1024)S(1)}, f32[2048]{0:T(1024)}, u32[]{:S(2)}) copy-start(f32[2048]{0:T(1024)} %param.16) | copy-start | bytes 24580
  6.5 72.4 %all-gather.6.cloned.1.call-start = ((), (), s32[]{:S(2)}) async-start(), calls=%async_computation.1 | async-start | bytes 4718592 | tf_op jit(solution)/shard_map/all_gather | solution.py:49
  7.3 120.8 %all-gather.8.cloned.1.call-start = ((), (), s32[]{:S(2)}) async-start(), calls=%async_computation.2 | async-start | bytes 2359296 | tf_op jit(solution)/shard_map/all_gather | solution.py:63
  79.0 3.5 copy-start.1
  83.8 4.3 copy-start.3
  83.8 4.5 %copy-start.6 = (bf16[64,256]{1,0:T(8,128)(2,1)S(1)}, bf16[64,256]{1,0:T(8,128)(2,1)}, u32[]{:S(2)}) copy-start(bf16[64,256]{1,0:T(8,128)(2,1)} %param.22) | copy-start | bytes 98308
  85.1 45.2 %copy-start.13 = (f32[1024]{0:T(1024)S(1)}, f32[1024]{0:T(1024)}, u32[]{:S(2)}) copy-start(f32[1024]{0:T(1024)} %param.21) | copy-start | bytes 12292
  85.1 45.2 %copy-start.14 = (f32[1024]{0:T(1024)S(1)}, f32[1024]{0:T(1024)}, u32[]{:S(2)}) copy-start(f32[1024]{0:T(1024)} %param.20) | copy-start | bytes 12292
  88.0 85.7 %all-gather.10.cloned.1.call-start = ((), (), s32[]{:S(2)}) async-start(), calls=%async_computation.3 | async-start | bytes 4718592 | tf_op jit(solution)/shard_map/all_gather | solution.py:74
  130.4 4.6 %copy-start.4 = (bf16[128,704]{0,1:T(8,128)(2,1)S(1)}, bf16[128,704]{0,1:T(8,128)(2,1)}, u32[]{:S(2)}) copy-start(bf16[128,704]{0,1:T(8,128)(2,1)} %param.25) | copy-start | bytes 540676
  130.4 4.6 %copy-start.5 = (bf16[128,704]{0,1:T(8,128)(2,1)S(1)}, bf16[128,704]{0,1:T(8,128)(2,1)}, u32[]{:S(2)}) copy-start(bf16[128,704]{0,1:T(8,128)(2,1)} %param.24) | copy-start | bytes 540676
  130.4 6.3 %copy-start.7 = (f32[3,704]{1,0:T(4,128)S(1)}, f32[3,704]{1,0:T(4,128)}, u32[]{:S(2)}) copy-start(f32[3,704]{1,0:T(4,128)} %param.27) | copy-start | bytes 25348
  130.4 6.3 %copy-start.8 = (f32[3,704]{1,0:T(4,128)S(1)}, f32[3,704]{1,0:T(4,128)}, u32[]{:S(2)}) copy-start(f32[3,704]{1,0:T(4,128)} %param.26) | copy-start | bytes 25348
  134.8 135.8 %copy-start.12 = (f32[2048]{0:T(1024)S(1)}, f32[2048]{0:T(1024)}, u32[]{:S(2)}) copy-start(f32[2048]{0:T(1024)} %param.23) | copy-start | bytes 24580
  134.9 135.8 %all-gather.12.cloned.1.call-start = ((), (), s32[]{:S(2)}) async-start(), calls=%async_computation.4 | async-start | bytes 6127616 | tf_op jit(solution)/shard_map/all_gather | solution.py:13
  135.8 214.4 %all-gather.14.cloned.1.call-start = ((), (), s32[]{:S(2)}) async-start(), calls=%async_computation.5 | async-start | bytes 3063808 | tf_op jit(solution)/shard_map/all_gather | solution.py:84
  136.5 274.7 %reduce-scatter.2.cloned.1.call-start = ((), (), s32[]{:S(2)}) async-start(), calls=%async_computation.6 | async-start | bytes 4718592 | tf_op jit(solution)/shard_map/reduce_scatter | solution.py:87
  270.7 6.4 %copy-start.2 = (bf16[1024,2048]{0,1:T(8,128)(2,1)S(1)}, bf16[1024,2048]{0,1:T(8,128)(2,1)}, u32[]{:S(2)}) copy-start(bf16[1024,2048]{0,1:T(8,128)(2,1)} %all-gather.10.cloned.1.call-done) | copy-start | bytes 12582916
  270.7 6.5 %copy-start.10 = (bf16[2048,1408]{0,1:T(8,128)(2,1)S(1)}, bf16[2048,1408]{0,1:T(8,128)(2,1)}, u32[]{:S(2)}) copy-start(bf16[2048,1408]{0,1:T(8,128)(2,1)} %all-gather.12.cloned.1.call-done) | copy-start | bytes 17301508
  362.4 48.8 %copy-start = (bf16[1024,256]{0,1:T(8,128)(2,1)S(1)}, bf16[1024,256]{0,1:T(8,128)(2,1)}, u32[]{:S(2)}) copy-start(bf16[1024,256]{0,1:T(8,128)(2,1)} %fusion.36) | copy-start | bytes 1572868
  362.4 64.8 %copy-start.9 = (f32[256]{0:T(256)S(1)}, f32[256]{0:T(256)}, u32[]{:S(2)}) copy-start(f32[256]{0:T(256)} %param.29) | copy-start | bytes 3076
Sparse Core Ops, SparseCore 0:
  9.2 56.5 all-gather.5
  88.1 39.9 all-gather.7
  135.0 38.6 all-gather.9
  175.3 95.3 all-gather.11
  272.3 77.9 all-gather.13
  362.6 48.5 reduce-scatter.1
where the time goes:
time: 437 us; the launch traced here: 436 us
  waiting for transfers between devices  265 us (61%)
  blocking collectives  108 us (25%)
  matrix products  30.5 us (7%)
  other arithmetic  14.7 us (3%)
  between operations  13.7 us (3%)
    all_gather x1, waiting for transfers between devices, side_by_side(): lax.all_gather(both, axis, axis=dim, tiled=True)  93.9 us
    all_gather x1, waiting for transfers between devices, local(): lax.all_gather(mlp_down, 'fs', axis=1, tiled=True)  68.3 us
    reduce_scatter x1, waiting for transfers between devices, local(): lax.psum_scatter(partial_terms.astype(jnp.bfloat16), 'tp', scatter_dimens...  48.7 us
    all_gather x1, blocking collectives, local(): lax.all_gather(gate_proj, 'fs', axis=0, tiled=True)  46.4 us
    all_gather x1, waiting for transfers between devices, local(): whole_two = lax.all_gather(mixed, 'tp', axis=1, tiled=True)  36.9 us
    all_gather x1, blocking collectives, local(): lax.all_gather(mix_out, 'fs', axis=0, tiled=True)  23.6 us
    all_gather x1, blocking collectives, local(): lax.all_gather(value_proj, 'fs', axis=0, tiled=True)  23.2 us
    all_gather x1, waiting for transfers between devices, local(): lax.all_gather(conv_out, 'tp', axis=1, tiled=True).astype(jnp.float32)  16.1 us
  transfers between devices with their start and end apart: 6, of which 5 were waited for; matrix products, arithmetic and copies ran while one was open for 4% of the time, Pallas kernels for 0%

commit v1 on v0

v1 whole, which is shorter than its diff:
```python
import functools

import jax
import jax.numpy as jnp
from jax import lax
from jax.experimental import pallas as pl
from jax.experimental.pallas import tpu as pltpu
from jax.sharding import PartitionSpec as P

F32 = jnp.float32
BF16 = jnp.bfloat16
CHUNKS = 4
LANE = 128
PAD = 16
AB, CP, DP, CB0, CB1 = range(5)
TOK, CONV, MIX = range(3)


def body(
    sizes,
    tokens,
    mix_gain,
    value_own,
    gate_own,
    conv_taps,
    chan_gain,
    chan_shift,
    mix_out_own,
    mlp_gain,
    c_own,
    c_taps,
    d_own,
    final_gain,
    out,
    wab,
    wc,
    wd,
    tf,
    cf,
    mf,
    nrm,
    glu,
    gp,
    hm,
    hh,
    acc,
    qs,
    qr,
    fs_,
    fr,
    ns,
    nr,
    sm,
    ss_send,
    ss_recv,
    ob,
    lsem,
    zs,
    zr,
    ys,
    yr,
    xs,
    xr,
    rs,
    rr,
    ts,
    tr,
    osem,
):
    nf, nt = sizes
    nx = nt // 2
    half = nf // 2
    rows, fd = tokens.shape
    dm = tf.shape[1]
    ca = cf.shape[1]
    fc = ca // nt
    cr = rows // CHUNKS
    ffd = hh.shape[1]
    full_tiles = ffd // LANE * LANE
    tail = ffd - full_tiles
    kz = value_own.shape[0]
    kb = mix_out_own.shape[0]

    grp = lax.axis_index("grp")
    fs = lax.axis_index("fs")
    tp = lax.axis_index("tp")
    xi = tp // 2
    co = lax.rem(tp, 2)
    par = lax.rem(grp, 2)
    other = 1 - par

    def tp_of(dx, flip=False):
        core = 1 - co if flip else co
        return lax.rem(xi + dx + nx, nx) * 2 + core

    def dev_tp(t):
        return (grp, fs, t)

    def dev_fs(d):
        return (grp, lax.rem(fs + d + nf, nf), tp)

    peer_y = (grp + 1 - 2 * par, fs, tp)
    right, left, partner = dev_tp(tp_of(1)), dev_tp(tp_of(-1)), dev_tp(tp_of(0, True))
    zdev = (dev_fs(1), dev_fs(-1))

    def remote(src, dst, ssem, rsem, dev):
        return pltpu.make_async_remote_copy(
            src_ref=src,
            dst_ref=dst,
            send_sem=ssem,
            recv_sem=rsem,
            device_id=dev,
            device_id_type=pl.DeviceIdType.MESH,
        )

    sends = []

    def send(ref, ssem, rsem, dev, dst=None):
        copy = remote(ref, ref if dst is None else dst, ssem, rsem, dev)
        copy.start()
        sends.append(copy)

    def landed(ref, sem):
        remote(ref, ref, sem, sem, partner).wait_recv()

    def own_c(r0, n):
        return wc.at[fs, pl.ds(r0, n)]

    tok_cols = pl.ds(pl.multiple_of(tp * fd, fd), fd)
    moves = [
        (value_own, wab.at[fs, pl.ds(0, kz)]),
        (gate_own, wab.at[fs, pl.ds(kz, kz)]),
        (mix_out_own.at[:, pl.ds(0, LANE)], wab.at[fs, pl.ds(2 * kz, kb)]),
        (mix_out_own.at[:, pl.ds(LANE, LANE)], wab.at[fs, pl.ds(2 * kz + kb, kb)]),
        (tokens, tf.at[:, tok_cols]),
        (c_own, wc.at[fs]),
        (d_own, wd.at[fs]),
    ]
    local = [pltpu.make_async_copy(a, b, lsem.at[i]) for i, (a, b) in enumerate(moves)]
    for copy in local:
        copy.start()

    barrier = pltpu.get_barrier_semaphore()
    peers = [dev_tp(lax.rem(tp + o, nt)) for o in range(1, nt)] + [zdev[0], zdev[1], peer_y]
    for dev in peers:
        pl.semaphore_signal(barrier, inc=1, device_id=dev, device_id_type=pl.DeviceIdType.MESH)

    glu[pl.ds(0, PAD), :] = jnp.zeros((PAD, fc), F32)
    glu[pl.ds(PAD + rows, PAD), :] = jnp.zeros((PAD, fc), F32)
    gp[pl.ds(0, PAD), :] = jnp.zeros((PAD, gp.shape[1]), F32)
    gp[pl.ds(PAD + rows, PAD), :] = jnp.zeros((PAD, gp.shape[1]), F32)
    for copy in local:
        copy.wait()
    pl.semaphore_wait(barrier, len(peers))

    quarter = kz // 4
    dhalf = ffd // 2

    def zslice(lane, idx, h=None, who=None):
        who = par if who is None else who
        if lane == AB:
            ref, r0, n, step = wab, 0, wab.shape[1], 8
        elif lane == CP:
            ref, r0, n, step = wc, 2 * quarter + who * quarter, quarter, quarter
        elif lane == CB0:
            ref, r0, n, step = wc, 0, quarter, quarter
        elif lane == CB1:
            ref, r0, n, step = wc, quarter, quarter, quarter
        else:
            ref, r0, n, step = wd, who * dhalf, dhalf, dhalf
        if h is not None:
            r0, n = r0 + h * (n // 2), n // 2
        if not isinstance(r0, int):
            r0 = pl.multiple_of(r0, 16)
        return ref.at[idx, pl.ds(r0, n)]

    ylane = {CP: 0, DP: 1}

    def zidx(s, d):
        return lax.rem(fs - s + nf, nf) if d == 0 else lax.rem(fs + s, nf)

    def ymsg(s, d):
        return 2 * (s - 1) + d

    def z_own(lane):
        for d in range(2):
            send(zslice(lane, fs), zs.at[lane, 0, d], zr.at[lane, 1, d], zdev[d])

    def z_visit(lane, s):
        h = [None, None] if s < half else [0, 1]
        for d in range(2):
            idx = zidx(s, d)
            landed(zslice(lane, idx, h[d]), zr.at[lane, s, d])
            if s < half:
                piece = zslice(lane, idx, d if s == half - 1 else None)
                send(piece, zs.at[lane, s, d], zr.at[lane, s + 1, d], zdev[d])
        if lane in ylane:
            y = ylane[lane]
            for d in range(2):
                m = ymsg(s, d)
                send(zslice(lane, zidx(s, d), h[d]), ys.at[y, m], yr.at[y, m], peer_y)

    def y_done(lane):
        y = ylane[lane]
        for s in range(1, half + 1):
            for d in range(2):
                h = d if s == half else None
                landed(zslice(lane, zidx(s, d), h, other), yr.at[y, ymsg(s, d)])

    first, second = (AB, CP), (DP, CB0, CB1)
    visits = [(lane, s) for s in range(1, half + 1) for lane in first]
    visits += [(lane, s) for s in range(1, half + 1) for lane in second]
    queue = list(visits)

    def pump(n):
        for _ in range(min(n, len(queue))):
            lane, s = queue.pop(0)
            z_visit(lane, s)
            if (lane, s) == (first[-1], half - 1):
                for follow in second:
                    z_own(follow)

    def pump_to(lane, s):
        while (lane, s) in queue:
            pump(1)

    bufs = (tf, cf, mf)

    def blk(k, r, t, h=None):
        width = fc if k == CONV else fd
        r0, n = r * cr, cr
        if h is not None:
            r0, n = r0 + h * (cr // 2), cr // 2
        return bufs[k].at[pl.ds(r0, n), pl.ds(pl.multiple_of(t * width, width), width)]

    def ag_own(k, r):
        mine = blk(k, r, tp)
        send(mine, xs.at[k, r, 0], xr.at[k, r, 0], right)
        send(mine, xs.at[k, r, 1], xr.at[k, r, 1], left)
        send(mine, xs.at[k, r, 4], xr.at[k, r, 4], partner)

    def ag_v1(k, r):
        for d, (src, onward) in enumerate(((tp_of(-1), right), (tp_of(1), left))):
            landed(blk(k, r, src), xr.at[k, r, d])
            send(blk(k, r, src, d), xs.at[k, r, 2 + d], xr.at[k, r, 2 + d], onward)
            send(blk(k, r, src), xs.at[k, r, 5 + d], xr.at[k, r, 5 + d], partner)

    def ag_v2(k, r):
        for d in range(2):
            piece = blk(k, r, tp_of(2), d)
            landed(piece, xr.at[k, r, 2 + d])
            send(piece, xs.at[k, r, 7 + d], xr.at[k, r, 7 + d], partner)

    def ag_done(k, r):
        landed(blk(k, r, tp_of(0, True)), xr.at[k, r, 4])
        landed(blk(k, r, tp_of(-1, True)), xr.at[k, r, 5])
        landed(blk(k, r, tp_of(1, True)), xr.at[k, r, 6])
        landed(blk(k, r, tp_of(2, True), 0), xr.at[k, r, 7])
        landed(blk(k, r, tp_of(2, True), 1), xr.at[k, r, 8])

    tile = min(128, cr)

    def tiles(r, n, fn):
        def step(i, carry):
            fn(pl.multiple_of(r * cr + i * n, n))
            return carry

        lax.fori_loop(0, cr // n, step, 0)

    def norm(src, gain, r):
        def one(r0):
            total = jnp.zeros((tile, LANE), F32)
            for j in range(dm // LANE):
                v = src[pl.ds(r0, tile), pl.ds(j * LANE, LANE)].astype(F32)
                total = total + v * v
            scale = lax.rsqrt(jnp.sum(total, axis=-1, keepdims=True) / dm + 1e-06)
            for j in range(dm // LANE):
                cols = pl.ds(j * LANE, LANE)
                v = src[pl.ds(r0, tile), cols].astype(F32)
                nrm[pl.ds(r0, tile), cols] = (v * scale * gain[:, cols]).astype(BF16)

        tiles(r, tile, one)

    def mat_a(r):
        w = jnp.concatenate(
            [
                wab[:, 0:kz, :].reshape(dm, fc),
                wab[:, kz : 2 * kz, :].reshape(dm, fc),
            ],
            axis=1,
        )
        both = jnp.dot(nrm[pl.ds(r * cr, cr), :], w, preferred_element_type=F32)
        v, g = both[:, :fc], both[:, fc:]
        glu[pl.ds(PAD + r * cr, cr), :] = v / (1.0 + jnp.exp(-g))

    def conv(r):
        width = conv_taps.shape[0]
        base = PAD - (width - 1) // 2
        n = min(64, cr)

        def one(r0):
            total = jnp.zeros((n, fc), F32)
            for k in range(width):
                total = total + conv_taps[k : k + 1, :] * glu[pl.ds(r0 + base + k, n), :]
            cf[pl.ds(r0, n), pl.ds(pl.multiple_of(tp * fc, fc), fc)] = total.astype(BF16)

        tiles(r, n, one)

    def mix(r):
        def one(r0):
            s1 = jnp.zeros((tile, LANE), F32)
            s2 = jnp.zeros((tile, LANE), F32)
            for j in range(ca // LANE):
                v = cf[pl.ds(r0, tile), pl.ds(j * LANE, LANE)].astype(F32)
                s1 = s1 + v
                s2 = s2 + v * v
            mean = jnp.sum(s1, axis=-1, keepdims=True) / ca
            var = jnp.sum(s2, axis=-1, keepdims=True) / ca - mean * mean
            inv = lax.rsqrt(var + 1e-05)
            for j in range(ca // LANE):
                cols = pl.ds(j * LANE, LANE)
                v = cf[pl.ds(r0, tile), cols].astype(F32)
                v = (v - mean) * inv * chan_gain[:, cols] + chan_shift[:, cols]
                hm[pl.ds(r0, tile), cols] = (v / (1.0 + jnp.exp(-v))).astype(BF16)

        tiles(r, tile, one)
        w = jnp.concatenate(
            [
                wab[:, 2 * kz : 2 * kz + kb, :].reshape(ca, LANE),
                wab[:, 2 * kz + kb :, :].reshape(ca, LANE),
            ],
            axis=1,
        )
        here = pl.ds(r * cr, cr)
        prod = jnp.dot(hm[here, :], w, preferred_element_type=F32)
        mf[here, tok_cols] = (tf[here, tok_cols].astype(F32) + prod).astype(BF16)

    def mat_c(r):
        w = wc[...].reshape(dm, wc.shape[2])
        gp[pl.ds(PAD + r * cr, cr), :] = jnp.dot(
            nrm[pl.ds(r * cr, cr), :], w, preferred_element_type=F32
        )

    def hidden(r):
        n = min(64, cr)

        def conv3(r0, cols):
            window = gp[pl.ds(pl.multiple_of(r0 + PAD - 8, 8), n + 16), cols]
            total = c_taps[0:1, cols] * window[7 : 7 + n]
            for k in range(1, c_taps.shape[0]):
                total = total + c_taps[k : k + 1, cols] * window[7 + k : 7 + k + n]
            return total

        def one(r0):
            for j in range(full_tiles // LANE):
                g = conv3(r0, pl.ds(j * LANE, LANE))
                u = conv3(r0, pl.ds(full_tiles + j * LANE, LANE))
                hh[pl.ds(r0, n), pl.ds(j * LANE, LANE)] = (g / (1.0 + jnp.exp(-g)) * u).astype(BF16)
            v = conv3(r0, pl.ds(2 * full_tiles, LANE))
            u = pltpu.roll(v, LANE - tail, 1)
            h = (v / (1.0 + jnp.exp(-v)) * u).astype(BF16)
            hh[pl.ds(r0, n), pl.ds(full_tiles, tail)] = h[:, :tail]

        tiles(r, n, one)

    def down(r, m):
        w = jnp.concatenate([wd[2 * m], wd[2 * m + 1]], axis=1)
        return jnp.dot(hh[pl.ds(r * cr, cr), :], w, preferred_element_type=F32)

    hr = cr // 2

    def rs_a(r):
        for q in range(nx):
            qs[r, q] = down(r, 2 * q + 1 - co).astype(BF16)
        send(qs.at[r], rs.at[r, 0], rr.at[r, 0], partner, qr.at[r])
        for q in range(nx):
            acc[r, q] = down(r, 2 * q + co)

    xr1, xl1, xo = lax.rem(xi + 1, nx), lax.rem(xi + nx - 1, nx), lax.rem(xi + 2, nx)

    def rs_b(r):
        landed(qr.at[r], rr.at[r, 0])
        far = acc[r, xo] + qr[r, xo].astype(F32)
        fs_[r] = far.astype(BF16)
        send(fs_.at[r, pl.ds(0, hr)], rs.at[r, 1], rr.at[r, 1], right, fr.at[r, pl.ds(0, hr)])
        send(fs_.at[r, pl.ds(hr, hr)], rs.at[r, 2], rr.at[r, 2], left, fr.at[r, pl.ds(hr, hr)])

    def rs_c(r):
        for d, (q, onward) in enumerate(((xr1, right), (xl1, left))):
            landed(fr.at[r, pl.ds(d * hr, hr)], rr.at[r, 1 + d])
            gets, keeps = pl.ds(d * hr, hr), pl.ds((1 - d) * hr, hr)
            both = acc[r, q, gets] + qr[r, q, gets].astype(F32) + fr[r, gets].astype(F32)
            ns[r, d, gets] = both.astype(BF16)
            ns[r, d, keeps] = (acc[r, q, keeps] + qr[r, q, keeps].astype(F32)).astype(BF16)
            send(ns.at[r, d], rs.at[r, 3 + d], rr.at[r, 3 + d], onward, nr.at[r, d])

    def rs_d(r):
        here = pl.ds(r * cr, cr)
        total = acc[r, xi] + qr[r, xi].astype(F32) + mf[here, tok_cols].astype(F32)
        for d in range(2):
            landed(nr.at[r, d], rr.at[r, 3 + d])
        total = total + nr[r, 0].astype(F32) + nr[r, 1].astype(F32)
        sm[here, :] = total
        part = jnp.sum(total * total, axis=-1, keepdims=True)
        ss_send[r] = jnp.transpose(jnp.broadcast_to(part, (cr, LANE)))[0:8, :]
        for o in range(1, nt):
            send(
                ss_send.at[r],
                ts.at[r, o],
                tr.at[r, o],
                dev_tp(lax.rem(tp + o, nt)),
                ss_recv.at[r, o],
            )

    def rs_e(r):
        here = pl.ds(r * cr, cr)
        total = ss_send[r]
        for o in range(1, nt):
            landed(ss_recv.at[r, o], tr.at[r, o])
        for o in range(1, nt):
            total = total + ss_recv[r, o]
        wide = jnp.broadcast_to(total[0:1, :], (LANE, cr))
        scale = lax.rsqrt(jnp.transpose(wide)[:, 0:1] / dm + 1e-06)
        ob[here, :] = (sm[here, :] * scale * final_gain[...]).astype(BF16)
        pltpu.make_async_copy(ob.at[here, :], out.at[here, :], osem.at[r]).start()

    z_own(AB)
    z_own(CP)
    ag_own(TOK, 0)
    ag_own(TOK, 1)
    for r in range(CHUNKS):
        ag_v1(TOK, r)
        if r + 2 < CHUNKS:
            ag_own(TOK, r + 2)
        pump(1)
        if r >= 1:
            ag_v2(TOK, r - 1)
            ag_done(TOK, r - 1)
            norm(tf, mix_gain, r - 1)
        pump(1)
    ag_v2(TOK, CHUNKS - 1)
    ag_done(TOK, CHUNKS - 1)
    norm(tf, mix_gain, CHUNKS - 1)
    pump_to(AB, half)
    for r in range(CHUNKS):
        mat_a(r)
        if r >= 1:
            conv(r - 1)
            ag_own(CONV, r - 1)
        if r == 1:
            pump(1)
    conv(CHUNKS - 1)
    ag_own(CONV, CHUNKS - 1)
    pump(1)
    ag_v1(CONV, 0)
    ag_v1(CONV, 1)
    for r in range(CHUNKS):
        pump(1)
        ag_v2(CONV, r)
        if r + 2 < CHUNKS:
            ag_v1(CONV, r + 2)
        ag_done(CONV, r)
        mix(r)
        ag_own(MIX, r)
    pump(1)
    ag_v1(MIX, 0)
    pump(1)
    ag_v1(MIX, 1)
    for r in range(CHUNKS):
        pump(1)
        ag_v2(MIX, r)
        if r + 2 < CHUNKS:
            ag_v1(MIX, r + 2)
        pump(1)
        ag_done(MIX, r)
        norm(mf, mlp_gain, r)
    pump(len(queue))
    y_done(CP)
    last = CHUNKS - 1
    stages = (mat_c, None, hidden, rs_a, rs_b, rs_c, rs_d, rs_e)
    for tick in range(CHUNKS + len(stages) - 1):
        for lag in reversed(range(len(stages))):
            r = tick - lag
            if 0 <= r <= last and stages[lag] is not None:
                if lag == 3 and r == 0:
                    y_done(DP)
                stages[lag](r)

    for r in range(CHUNKS):
        here = pl.ds(r * cr, cr)
        pltpu.make_async_copy(ob.at[here, :], out.at[here, :], osem.at[r]).wait()
    for copy in sends:
        copy.wait_send()


def local(mesh, *args):
    (
        tokens,
        mix_gain,
        value_proj,
        gate_proj,
        conv_taps,
        chan_gain,
        chan_shift,
        mix_out,
        mlp_gain,
        mlp_gate,
        mlp_up,
        gate_taps,
        up_taps,
        mlp_down,
        final_gain,
    ) = args
    nf, nt = mesh.shape["fs"], mesh.shape["tp"]
    nx = nt // 2
    rows, fd = tokens.shape
    dm = mix_gain.shape[0]
    ca = chan_gain.shape[0]
    fc = value_proj.shape[1]
    kz, ffd = mlp_gate.shape
    kb = mix_out.shape[0]
    cr = rows // CHUNKS
    cut = ffd // LANE * LANE
    half = nf // 2

    def side(a, b):
        return jnp.concatenate([a[:, :cut], b[:, :cut], a[:, cut:], b[:, cut:]], axis=1)

    row = lambda v: v.reshape(1, -1)
    hbm = pl.BlockSpec(memory_space=pltpu.HBM)
    vmem = pl.BlockSpec(memory_space=pltpu.VMEM)
    dma = pltpu.SemaphoreType.DMA
    ny = 2 * half
    return pl.pallas_call(
        functools.partial(body, (nf, nt)),
        out_shape=jax.ShapeDtypeStruct((rows, fd), BF16),
        in_specs=[hbm, vmem, hbm, hbm, vmem, vmem, vmem, hbm, vmem, hbm, vmem, hbm, vmem],
        out_specs=hbm,
        scratch_shapes=[
            pltpu.VMEM((nf, 2 * kz + 2 * kb, LANE), BF16),
            pltpu.VMEM((nf, kz, 2 * ffd), BF16),
            pltpu.VMEM((nf, ffd, mlp_down.shape[1]), BF16),
            pltpu.VMEM((rows, dm), BF16),
            pltpu.VMEM((rows, ca), BF16),
            pltpu.VMEM((rows, dm), BF16),
            pltpu.VMEM((rows, dm), BF16),
            pltpu.VMEM((rows + 2 * PAD, fc), F32),
            pltpu.VMEM((rows + 2 * PAD, 2 * ffd), F32),
            pltpu.VMEM((rows, ca), BF16),
            pltpu.VMEM((rows, ffd), BF16),
            pltpu.VMEM((CHUNKS, nx, cr, fd), F32),
            pltpu.VMEM((CHUNKS, nx, cr, fd), BF16),
            pltpu.VMEM((CHUNKS, nx, cr, fd), BF16),
            pltpu.VMEM((CHUNKS, cr, fd), BF16),
            pltpu.VMEM((CHUNKS, cr, fd), BF16),
            pltpu.VMEM((CHUNKS, 2, cr, fd), BF16),
            pltpu.VMEM((CHUNKS, 2, cr, fd), BF16),
            pltpu.VMEM((rows, fd), F32),
            pltpu.VMEM((CHUNKS, 8, cr), F32),
            pltpu.VMEM((CHUNKS, nt, 8, cr), F32),
            pltpu.VMEM((rows, fd), BF16),
            dma((7,)),
            dma((5, half + 1, 2)),
            dma((5, half + 1, 2)),
            dma((2, ny)),
            dma((2, ny)),
            dma((3, CHUNKS, 9)),
            dma((3, CHUNKS, 9)),
            dma((CHUNKS, 5)),
            dma((CHUNKS, 5)),
            dma((CHUNKS, nt)),
            dma((CHUNKS, nt)),
            dma((CHUNKS,)),
        ],
        compiler_params=pltpu.CompilerParams(
            collective_id=0, has_side_effects=True, vmem_limit_bytes=67043328
        ),
        name="layer",
    )(
        tokens,
        row(mix_gain),
        value_proj,
        gate_proj,
        conv_taps,
        row(chan_gain),
        row(chan_shift),
        mix_out,
        row(mlp_gain),
        side(mlp_gate, mlp_up),
        side(gate_taps, up_taps),
        mlp_down,
        row(final_gain),
    )


def solution(mesh):
    return jax.shard_map(
        functools.partial(local, mesh),
        mesh=mesh,
        in_specs=(
            P(("grp", "fs"), "tp"),
            P(),
            P("fs", "tp"),
            P("fs", "tp"),
            P(None, "tp"),
            P(),
            P(),
            P("fs", "tp"),
            P(),
            P("fs", "tp"),
            P("fs", "tp"),
            P(None, "tp"),
            P(None, "tp"),
            P("tp", "fs"),
            P("tp"),
        ),
        out_specs=P(("grp", "fs"), "tp"),
        check_vma=False,
    )
```

time: 437 us -> 169 us (0.39)
  waiting for transfers between devices: 265 us -> 0 us
  Pallas kernels: 0 us -> 161 us
  blocking collectives: 108 us -> 0 us
  matrix products: 30.5 us -> 0 us
  other arithmetic: 14.7 us -> 0 us
  between operations: 13.7 us -> 0.06 us
  local copies, waits for them, and re-layouts: 3.5 us -> 7.93 us
    all_gather x5 -> x0, waiting for transfers between devices: 215 us -> none  [the longest x1 93.9 us: side_by_side(): lax.all_gather(both, axis, axis=dim, tiled=True)]
    pallas_call x0 -> x1, Pallas kernels: none -> 161 us  [local(): pl.pallas_call(functools.partial(body, (nf, nt)), out_shape=jax.ShapeDtyp...]
    all_gather x3 -> x0, blocking collectives: 93.3 us -> none  [the longest x1 46.4 us: local(): lax.all_gather(gate_proj, 'fs', axis=0, tiled=True)]
    reduce_scatter x1 -> x0, waiting for transfers between devices: 48.7 us -> none  [local(): lax.psum_scatter(partial_terms.astype(jnp.bfloat16), 'tp', scatter_dimens...]
    dot_general x6 -> x0, matrix products: 30.5 us -> none  [the longest x1 12.2 us: local(): jnp.dot(hidden_mlp, lax.all_gather(mlp_down, 'fs', axis=1, tiled=True), p...]
    psum x1 -> x0, blocking collectives: 14.8 us -> none  [local(): squares = lax.psum(jnp.sum(summed * summed, axis=-1, keepdims=True), 'tp')]
    reduce_sum x4 -> x0, other arithmetic: 9.83 us -> none  [the longest x2 6.33 us: rms_scale(): jnp.mean(values * values, axis=-1, keepdims=True) + 1e-06]
  transfers between devices with their start and end apart: 6 -> 0, of which waited for: 5 -> 0; matrix products, arithmetic and copies ran while one was open for 4% -> 0% of each run, Pallas kernels for 0% -> 0%
where the time goes in v1:
time: 169 us
  Pallas kernels  161 us (95%)
  local copies, waits for them, and re-layouts  7.93 us (5%)
    pallas_call x1, Pallas kernels, local(): pl.pallas_call(functools.partial(body, (nf, nt)), out_shape=jax.ShapeDtyp...  161 us

profile of v1, /device:TPU:33, one launch (start us, length us, event | category | flops | bytes accessed | tf_op | source)
XLA Modules:
  0.0 168.5 jit_solution(18376350126644227771)
XLA Ops:
  0.0 0.0 slice-start.7
  0.0 0.0 slice-start.4
  0.0 0.0 slice-start.5
  0.0 0.0 slice-start.6
  0.0 0.7 slice-done.7
  0.7 0.0 slice-done.4
  0.7 0.0 slice-done.5
  0.7 0.0 slice-done.6
  0.7 0.7 concatenate.7.c_taps
  1.4 0.0 slice-start
  1.4 0.7 slice-done
  2.1 0.1 copy.22
  2.3 0.0 slice-start.2
  2.3 0.7 slice-done.2
  3.0 0.1 copy.23
  3.1 0.0 slice-start.1
  3.1 0.9 slice-done.1
  4.0 0.2 copy.20
  4.2 0.0 slice-start.3
  4.2 0.9 slice-done.3
  5.1 0.2 copy.21
  5.3 0.8 concatenate.6.c_own
  6.1 160.5 %layer.1 = bf16[1024,256]{1,0:T(8,128)(2,1)} custom-call(bf16[1024,256]{1,0:T(8,128)(2,1)} %tokens.1, f32[1,2048]{1,0:T(1,128)} %bitcast.5, bf16[128,128]{1,0:T(8,128)(2,1)} %value_own.1, bf16[128,128]{1,0:T(8,128)(2,1)} %gate_own.1, f32[31,128]{1,0:T(8,128)} %conv_taps.1, f32[1,1024]{1,0:T(1,128)} %bitcast.7, f32[1,1024]{1,0:T(1,128)} %bitcast.8, ...), custom_call_target="tpu_custom_call" | custom-call | tf_op jit(solution)/shard_map/layer/pallas_call | solution.py:534
  166.6 1.9 %copy.25 = bf16[1024,256]{1,0:T(8,128)(2,1)} copy(bf16[1024,256]{1,0:T(8,128)(2,1)} %layer.1) | data formatting | bytes 1048576
Async XLA Ops:
  0.0 0.7 slice-start.7
  0.0 0.7 slice-start.4
  0.0 0.7 slice-start.5
  0.0 0.7 slice-start.6
  1.4 0.7 slice-start
  2.3 0.7 slice-start.2
  3.1 0.9 slice-start.1
  4.2 0.9 slice-start.3

commit v2 on v1

v2 whole, which is shorter than its diff:
```python
import functools

import jax
import jax.numpy as jnp
from jax import lax
from jax.experimental import pallas as pl
from jax.experimental.pallas import tpu as pltpu
from jax.sharding import PartitionSpec as P

F32 = jnp.float32
BF16 = jnp.bfloat16
CHUNKS = 4
RCHUNKS = 8
LANE = 128
PAD = 16
EACH = 3
VAL, GAT, OUT, CP0, CX, CP1, CA, CB, DA, DB = range(10)
TOK, CONV, MIX = range(3)


def body(
    sizes,
    tokens,
    mix_gain,
    value_own,
    gate_own,
    conv_taps,
    chan_gain,
    chan_shift,
    mix_out_own,
    mlp_gain,
    mlp_gate,
    mlp_up,
    gate_taps,
    up_taps,
    d_own,
    final_gain,
    out,
    wab,
    wc,
    wd,
    tf,
    cf,
    mf,
    nrm,
    glu,
    gp,
    hm,
    hh,
    acc,
    qs,
    qr,
    fs_,
    fr,
    ns,
    nr,
    sm,
    ss_send,
    ss_recv,
    gbuf,
    ubuf,
    c_taps,
    lsem,
    zs,
    zr,
    ys,
    yr,
    xs,
    xr,
    rs,
    rr,
    ts,
    tr,
):
    nf, nt = sizes
    nx = nt // 2
    half = nf // 2
    rows, fd = tokens.shape
    dm = tf.shape[1]
    ca = cf.shape[1]
    fc = ca // nt
    cr = rows // CHUNKS
    ffd = hh.shape[1]
    full_tiles = ffd // LANE * LANE
    tail = ffd - full_tiles
    kz = value_own.shape[0]
    kb = mix_out_own.shape[0]

    grp = lax.axis_index("grp")
    fs = lax.axis_index("fs")
    tp = lax.axis_index("tp")
    xi = tp // 2
    co = lax.rem(tp, 2)
    par = lax.rem(grp, 2)
    other = 1 - par

    def tp_of(dx, flip=False):
        core = 1 - co if flip else co
        return lax.rem(xi + dx + nx, nx) * 2 + core

    def dev_tp(t):
        return (grp, fs, t)

    def dev_fs(d):
        return (grp, lax.rem(fs + d + nf, nf), tp)

    peer_y = (grp + 1 - 2 * par, fs, tp)
    right, left, partner = dev_tp(tp_of(1)), dev_tp(tp_of(-1)), dev_tp(tp_of(0, True))
    zdev = (dev_fs(1), dev_fs(-1))

    def remote(src, dst, ssem, rsem, dev):
        return pltpu.make_async_remote_copy(
            src_ref=src,
            dst_ref=dst,
            send_sem=ssem,
            recv_sem=rsem,
            device_id=dev,
            device_id_type=pl.DeviceIdType.MESH,
        )

    def send(ref, ssem, rsem, dev, dst=None):
        remote(ref, ref if dst is None else dst, ssem, rsem, dev).start()

    def landed(ref, sem):
        remote(ref, ref, sem, sem, partner).wait_recv()

    def left_here(ref, sem):
        remote(ref, ref, sem, sem, partner).wait_send()

    def own_c(r0, n):
        return wc.at[fs, pl.ds(r0, n)]

    tok_cols = pl.ds(pl.multiple_of(tp * fd, fd), fd)
    moves = [
        (value_own, wab.at[fs, pl.ds(0, kz)]),
        (gate_own, wab.at[fs, pl.ds(kz, kz)]),
        (mix_out_own.at[:, pl.ds(0, LANE)], wab.at[fs, pl.ds(2 * kz, kb)]),
        (mix_out_own.at[:, pl.ds(LANE, LANE)], wab.at[fs, pl.ds(2 * kz + kb, kb)]),
        (tokens, tf.at[:, tok_cols]),
        (mlp_gate, gbuf),
        (mlp_up, ubuf),
        (d_own, wd.at[fs]),
    ]
    local = [pltpu.make_async_copy(a, b, lsem.at[i]) for i, (a, b) in enumerate(moves)]
    for copy in local:
        copy.start()

    barrier = pltpu.get_barrier_semaphore()
    peers = [dev_tp(lax.rem(tp + o, nt)) for o in range(1, nt)] + [zdev[0], zdev[1], peer_y]
    for dev in peers:
        pl.semaphore_signal(barrier, inc=1, device_id=dev, device_id_type=pl.DeviceIdType.MESH)

    whole = full_tiles // LANE
    cut = EACH * LANE
    at = 0
    for taps, lo, hi in (
        (gate_taps, 0, cut),
        (up_taps, 0, cut),
        (gate_taps, cut, full_tiles),
        (up_taps, cut, full_tiles),
        (gate_taps, full_tiles, ffd),
        (up_taps, full_tiles, ffd),
    ):
        c_taps[0 : taps.shape[0], at : at + hi - lo] = taps[:, lo:hi]
        at += hi - lo

    def pack(pos):
        if pos == 2 * whole:
            piece = jnp.concatenate([gbuf[full_tiles:, :], ubuf[full_tiles:, :]], axis=0)
        else:
            if pos < 2 * EACH:
                src, j = (gbuf, pos) if pos < EACH else (ubuf, pos - EACH)
            else:
                src, j = (gbuf, pos - EACH) if pos < EACH + whole else (ubuf, pos - whole)
            piece = src[j * LANE : (j + 1) * LANE, :]
        turned = jnp.transpose(piece.astype(F32)).astype(BF16)
        wc[fs, :, pos * LANE : (pos + 1) * LANE] = turned

    for i in (5, 6):
        local[i].wait()
    soon = (0, EACH, 2 * EACH)
    for pos in soon:
        pack(pos)

    glu[pl.ds(0, PAD), :] = jnp.zeros((PAD, fc), F32)
    glu[pl.ds(PAD + rows, PAD), :] = jnp.zeros((PAD, fc), F32)
    gp[pl.ds(0, PAD), :] = jnp.zeros((PAD, gp.shape[1]), F32)
    gp[pl.ds(PAD + rows, PAD), :] = jnp.zeros((PAD, gp.shape[1]), F32)
    for i, copy in enumerate(local):
        if i not in (5, 6):
            copy.wait()
    pl.semaphore_wait(barrier, len(peers))

    dhalf = ffd // 2
    lanes = {
        VAL: (wab, (0, kz), None),
        GAT: (wab, (kz, kz), None),
        OUT: (wab, (2 * kz, 2 * kb), None),
        CP0: (wc, None, (0, 1)),
        CX: (wc, None, (2 * EACH, 1)),
        CP1: (wc, None, (1, EACH - 1)),
        CA: (wc, None, (2 * EACH + 1, 2)),
        CB: (wc, None, (2 * EACH + 3, 2)),
        DA: (wd, (0, dhalf // 2), None),
        DB: (wd, (dhalf // 2, dhalf // 2), None),
    }
    ylane = {CP0: 0, CP1: 1, DA: 2, DB: 3}

    def zslice(lane, idx, h=None, who=None):
        who = par if who is None else who
        ref, span, cols = lanes[lane]
        r0, n = (0, ref.shape[1]) if span is None else span
        if lane in (DA, DB):
            r0 = pl.multiple_of(who * dhalf + r0, 16)
        if h is not None:
            r0, n = r0 + h * (n // 2), n // 2
        if not isinstance(r0, int):
            r0 = pl.multiple_of(r0, 8)
        if cols is None:
            return ref.at[idx, pl.ds(r0, n)]
        c0 = cols[0] * LANE
        if lane in (CP0, CP1):
            c0 = pl.multiple_of(who * (EACH * LANE) + c0, LANE)
        return ref.at[idx, pl.ds(r0, n), pl.ds(c0, cols[1] * LANE)]

    def zidx(s, d):
        return lax.rem(fs - s + nf, nf) if d == 0 else lax.rem(fs + s, nf)

    near = half // 2

    def z_own(lane):
        for d in range(2):
            send(zslice(lane, fs), zs.at[lane], zr.at[lane, 1, d], zdev[d])

    def z_visit(lane, s):
        h = [None, None] if s < half else [0, 1]
        for d in range(2):
            idx = zidx(s, d)
            landed(zslice(lane, idx, h[d]), zr.at[lane, s, d])
            if s < half:
                piece = zslice(lane, idx, d if s == half - 1 else None)
                send(piece, zs.at[lane], zr.at[lane, s + 1, d], zdev[d])
        if lane in ylane:
            y, part = ylane[lane], 0 if s <= near else 1
            for d in range(2):
                send(zslice(lane, zidx(s, d), h[d]), ys.at[y], yr.at[y, part], peer_y)

    def y_done(lane, part):
        count = 2 * near if part == 0 else nf - 1 - 2 * near
        landed(zslice(lane, pl.ds(0, count), None, other), yr.at[ylane[lane], part])

    phases = ((VAL, GAT, OUT, CP0, CX), (CP1, CA, CB, DA, DB))
    queue = [(lane, s) for group in phases for s in range(1, half + 1) for lane in group]

    def pump(n):
        for _ in range(min(n, len(queue))):
            lane, s = queue.pop(0)
            z_visit(lane, s)
            for now, later in zip(phases, phases[1:]):
                if s == half - 1 and lane == now[-1]:
                    for follow in later:
                        z_own(follow)

    def pump_to(lane, s):
        while (lane, s) in queue:
            pump(1)

    bufs = (tf, cf, mf)

    def blk(k, r, t, h=None):
        width = fc if k == CONV else fd
        r0, n = r * cr, cr
        if h is not None:
            r0, n = r0 + h * (cr // 2), cr // 2
        return bufs[k].at[pl.ds(r0, n), pl.ds(pl.multiple_of(t * width, width), width)]

    def ag_own(k, r):
        mine = blk(k, r, tp)
        send(mine, xs.at[k], xr.at[k, r, 0], right)
        send(mine, xs.at[k], xr.at[k, r, 1], left)
        send(mine, xs.at[k], xr.at[k, r, 4], partner)

    def ag_v1(k, r):
        for d, (src, onward) in enumerate(((tp_of(-1), right), (tp_of(1), left))):
            landed(blk(k, r, src), xr.at[k, r, d])
            send(blk(k, r, src, d), xs.at[k], xr.at[k, r, 2 + d], onward)
            send(blk(k, r, src), xs.at[k], xr.at[k, r, 4], partner)

    def ag_v2(k, r):
        for d in range(2):
            piece = blk(k, r, tp_of(2), d)
            landed(piece, xr.at[k, r, 2 + d])
            send(piece, xs.at[k], xr.at[k, r, 4], partner)

    def ag_done(k, r):
        width = fc if k == CONV else fd
        landed(bufs[k].at[pl.ds(r * cr, cr), pl.ds(0, nx * width)], xr.at[k, r, 4])

    tile = min(128, cr)

    def tiles(r, n, fn):
        def step(i, carry):
            fn(pl.multiple_of(r * cr + i * n, n))
            return carry

        lax.fori_loop(0, cr // n, step, 0)

    def norm(src, gain, r):
        def one(r0):
            total = jnp.zeros((tile, LANE), F32)
            for j in range(dm // LANE):
                v = src[pl.ds(r0, tile), pl.ds(j * LANE, LANE)].astype(F32)
                total = total + v * v
            scale = lax.rsqrt(jnp.sum(total, axis=-1, keepdims=True) / dm + 1e-06)
            for j in range(dm // LANE):
                cols = pl.ds(j * LANE, LANE)
                v = src[pl.ds(r0, tile), cols].astype(F32)
                nrm[pl.ds(r0, tile), cols] = (v * scale * gain[:, cols]).astype(BF16)

        tiles(r, tile, one)

    def mat_a(r):
        w = jnp.concatenate(
            [
                wab[:, 0:kz, :].reshape(dm, fc),
                wab[:, kz : 2 * kz, :].reshape(dm, fc),
            ],
            axis=1,
        )
        both = jnp.dot(nrm[pl.ds(r * cr, cr), :], w, preferred_element_type=F32)
        v, g = both[:, :fc], both[:, fc:]
        glu[pl.ds(PAD + r * cr, cr), :] = v / (1.0 + jnp.exp(-g))

    def conv(r):
        width = conv_taps.shape[0]
        base = PAD - (width - 1) // 2
        n = min(64, cr)

        def one(r0):
            total = jnp.zeros((n, fc), F32)
            for k in range(width):
                total = total + conv_taps[k : k + 1, :] * glu[pl.ds(r0 + base + k, n), :]
            cf[pl.ds(r0, n), pl.ds(pl.multiple_of(tp * fc, fc), fc)] = total.astype(BF16)

        tiles(r, n, one)

    def mix(r):
        def one(r0):
            s1 = jnp.zeros((tile, LANE), F32)
            s2 = jnp.zeros((tile, LANE), F32)
            for j in range(ca // LANE):
                v = cf[pl.ds(r0, tile), pl.ds(j * LANE, LANE)].astype(F32)
                s1 = s1 + v
                s2 = s2 + v * v
            mean = jnp.sum(s1, axis=-1, keepdims=True) / ca
            var = jnp.sum(s2, axis=-1, keepdims=True) / ca - mean * mean
            inv = lax.rsqrt(var + 1e-05)
            for j in range(ca // LANE):
                cols = pl.ds(j * LANE, LANE)
                v = cf[pl.ds(r0, tile), cols].astype(F32)
                v = (v - mean) * inv * chan_gain[:, cols] + chan_shift[:, cols]
                hm[pl.ds(r0, tile), cols] = (v / (1.0 + jnp.exp(-v))).astype(BF16)

        tiles(r, tile, one)
        w = jnp.concatenate(
            [
                wab[:, 2 * kz : 2 * kz + kb, :].reshape(ca, LANE),
                wab[:, 2 * kz + kb :, :].reshape(ca, LANE),
            ],
            axis=1,
        )
        here = pl.ds(r * cr, cr)
        prod = jnp.dot(hm[here, :], w, preferred_element_type=F32)
        mf[here, tok_cols] = (tf[here, tok_cols].astype(F32) + prod).astype(BF16)

    first_pairs = [(zidx(s, 0), zidx(s, 1)) for s in range(1, near + 1)]
    last_pairs = [(zidx(s, 0), zidx(s, 1)) for s in range(near + 1, half)] + [(fs, zidx(half, 0))]

    def pair_dots(r, pairs):
        here = pl.ds(r * cr, cr)
        total = None
        for pair in pairs:
            cols = [pl.ds(pl.multiple_of(i * kz, kz), kz) for i in pair]
            lhs = jnp.concatenate([nrm[here, c] for c in cols], axis=1)
            rhs = jnp.concatenate([wc[i] for i in pair], axis=0)
            term = jnp.dot(lhs, rhs, preferred_element_type=F32)
            total = term if total is None else total + term
        return total

    def mat_c(r):
        gp[pl.ds(PAD + r * cr, cr), :] = pair_dots(r, first_pairs)

    def mat_late(r):
        here = pl.ds(PAD + r * cr, cr)
        gp[here, :] = gp[here, :] + pair_dots(r, last_pairs)

    hr = rows // RCHUNKS
    hn = min(64, hr)

    def conv3(r0, at):
        cols = pl.ds(at * LANE, LANE)
        window = gp[pl.ds(pl.multiple_of(r0 + PAD - 8, 8), hn + 16), cols]
        total = c_taps[0:1, cols] * window[7 : 7 + hn]
        for k in range(1, gate_taps.shape[0]):
            total = total + c_taps[k : k + 1, cols] * window[7 + k : 7 + k + hn]
        return total

    def units(r0, j):
        g = conv3(r0, j if j < EACH else EACH + j)
        u = conv3(r0, EACH + j if j < EACH else whole + j)
        hh[pl.ds(r0, hn), pl.ds(j * LANE, LANE)] = (g / (1.0 + jnp.exp(-g)) * u).astype(BF16)

    def hidden(r):
        def step(i, carry):
            r0 = pl.multiple_of(r * hr + i * hn, hn)
            for j in range(whole):
                units(r0, j)
            v = conv3(r0, 2 * whole)
            u = pltpu.roll(v, LANE - tail, 1)
            h = (v / (1.0 + jnp.exp(-v)) * u).astype(BF16)
            hh[pl.ds(r0, hn), pl.ds(full_tiles, tail)] = h[:, :tail]
            return carry

        lax.fori_loop(0, hr // hn, step, 0)

    def down(r, m):
        w = jnp.concatenate([wd[2 * m], wd[2 * m + 1]], axis=1)
        return jnp.dot(hh[pl.ds(r * hr, hr), :], w, preferred_element_type=F32)

    hf = hr // 2

    def rs_a(r):
        for q in range(nx):
            qs[r, q] = down(r, 2 * q + 1 - co).astype(BF16)
        send(qs.at[r], rs.at[0], rr.at[r, 0], partner, qr.at[r])
        for q in range(nx):
            acc[r, q] = down(r, 2 * q + co)

    xr1, xl1, xo = lax.rem(xi + 1, nx), lax.rem(xi + nx - 1, nx), lax.rem(xi + 2, nx)

    def rs_b(r):
        landed(qr.at[r], rr.at[r, 0])
        far = acc[r, xo] + qr[r, xo].astype(F32)
        fs_[r] = far.astype(BF16)
        send(fs_.at[r, pl.ds(0, hf)], rs.at[1], rr.at[r, 1], right, fr.at[r, pl.ds(0, hf)])
        send(fs_.at[r, pl.ds(hf, hf)], rs.at[1], rr.at[r, 2], left, fr.at[r, pl.ds(hf, hf)])

    def rs_c(r):
        for d, (q, onward) in enumerate(((xr1, right), (xl1, left))):
            landed(fr.at[r, pl.ds(d * hf, hf)], rr.at[r, 1 + d])
            gets, keeps = pl.ds(d * hf, hf), pl.ds((1 - d) * hf, hf)
            both = acc[r, q, gets] + qr[r, q, gets].astype(F32) + fr[r, gets].astype(F32)
            ns[r, d, gets] = both.astype(BF16)
            ns[r, d, keeps] = (acc[r, q, keeps] + qr[r, q, keeps].astype(F32)).astype(BF16)
            send(ns.at[r, d], rs.at[2], rr.at[r, 3], onward, nr.at[r, d])

    def rs_d(r):
        here = pl.ds(r * hr, hr)
        total = acc[r, xi] + qr[r, xi].astype(F32) + mf[here, tok_cols].astype(F32)
        landed(nr.at[r], rr.at[r, 3])
        total = total + nr[r, 0].astype(F32) + nr[r, 1].astype(F32)
        sm[here, :] = total
        part = jnp.sum(total * total, axis=-1, keepdims=True)
        ss_send[r] = jnp.transpose(jnp.broadcast_to(part, (hr, LANE)))[0:8, :]
        for o in range(1, nt):
            send(
                ss_send.at[r],
                ts.at[0],
                tr.at[r],
                dev_tp(lax.rem(tp + o, nt)),
                ss_recv.at[r, o - 1],
            )

    def rs_e(r):
        here = pl.ds(r * hr, hr)
        total = ss_send[r]
        landed(ss_recv.at[r], tr.at[r])
        for o in range(nt - 1):
            total = total + ss_recv[r, o]
        wide = jnp.broadcast_to(total[0:1, :], (LANE, hr))
        scale = lax.rsqrt(jnp.transpose(wide)[:, 0:1] / dm + 1e-06)
        out[here, :] = (sm[here, :] * scale * final_gain[...]).astype(BF16)

    for lane in phases[0]:
        z_own(lane)
    ag_own(TOK, 0)
    ag_own(TOK, 1)
    for pos in range(2 * whole + 1):
        if pos not in soon:
            pack(pos)
    pump(5)
    ag_v1(TOK, 0)
    ag_own(TOK, 2)
    pump(5)
    ag_v1(TOK, 1)
    ag_own(TOK, 3)
    pump(5)
    ag_v2(TOK, 0)
    pump(3)
    ag_done(TOK, 0)
    norm(tf, mix_gain, 0)
    pump(2)
    ag_v1(TOK, 2)
    ag_v2(TOK, 1)
    pump(3)
    ag_done(TOK, 1)
    norm(tf, mix_gain, 1)
    pump(2)
    ag_v1(TOK, 3)
    pump(2)
    ag_v2(TOK, 2)
    pump(3)
    ag_done(TOK, 2)
    norm(tf, mix_gain, 2)
    ag_v2(TOK, 3)
    pump(3)
    ag_done(TOK, 3)
    norm(tf, mix_gain, 3)
    pump_to(GAT, half)
    mat_a(0)
    pump_to(CX, half)
    for r in range(1, CHUNKS):
        mat_a(r)
        conv(r - 1)
        ag_own(CONV, r - 1)
        pump(1)
    conv(CHUNKS - 1)
    ag_own(CONV, CHUNKS - 1)
    ag_v1(CONV, 0)
    pump(1)
    ag_v1(CONV, 1)
    pump(1)
    ag_v1(CONV, 2)
    pump(1)
    ag_v1(CONV, 3)
    pump(1)
    ag_v2(CONV, 0)
    ag_v2(CONV, 1)
    pump(1)
    for r in range(CHUNKS):
        ag_done(CONV, r)
        mix(r)
        ag_own(MIX, r)
        pump(1)
        if r + 2 < CHUNKS:
            ag_v2(CONV, r + 2)
    pump(1)
    for r in range(CHUNKS):
        pump(2)
        ag_v1(MIX, r)
    pump(1)
    for r in range(CHUNKS):
        ag_v2(MIX, r)
        pump(1)
    for r in range(CHUNKS):
        ag_done(MIX, r)
        norm(mf, mlp_gain, r)
        pump(1)
    pump_to(CB, near)
    y_done(CP0, 0)
    y_done(CP1, 0)
    for r in range(CHUNKS):
        mat_c(r)
        pump(2)
    pump(len(queue))
    y_done(CP0, 1)
    y_done(CP1, 1)
    stages = {2: hidden, 3: rs_a, 4: rs_b, 6: rs_c, 8: rs_d, 10: rs_e}
    per = cr // hr
    for tick in range(RCHUNKS + max(stages)):
        if tick % per == 0 and tick // per < CHUNKS:
            mat_late(tick // per)
        for lag in sorted(stages, reverse=True):
            r = tick - lag
            if 0 <= r < RCHUNKS:
                if lag == 3 and r == 0:
                    for lane in (DA, DB):
                        y_done(lane, 0)
                        y_done(lane, 1)
                stages[lag](r)

    for lane in lanes:
        left_here(zslice(lane, pl.ds(0, nf - 1)), zs.at[lane])
        if lane in ylane:
            left_here(zslice(lane, pl.ds(0, nf - 1)), ys.at[ylane[lane]])
    for k, width in ((TOK, fd), (CONV, fc), (MIX, fd)):
        left_here(bufs[k].at[:, pl.ds(0, (nt - 1) * width)], xs.at[k])
    for i, ref in enumerate((qs, fs_, ns)):
        left_here(ref, rs.at[i])
    left_here(ss_recv, ts.at[0])


def local(mesh, *args):
    (
        tokens,
        mix_gain,
        value_proj,
        gate_proj,
        conv_taps,
        chan_gain,
        chan_shift,
        mix_out,
        mlp_gain,
        mlp_gate,
        mlp_up,
        gate_taps,
        up_taps,
        mlp_down,
        final_gain,
    ) = args
    nf, nt = mesh.shape["fs"], mesh.shape["tp"]
    nx = nt // 2
    rows, fd = tokens.shape
    dm = mix_gain.shape[0]
    ca = chan_gain.shape[0]
    fc = value_proj.shape[1]
    kz, ffd = mlp_gate.shape
    kb = mix_out.shape[0]
    hr = rows // RCHUNKS
    half = nf // 2
    row = lambda v: v.reshape(1, -1)
    hbm = pl.BlockSpec(memory_space=pltpu.HBM)
    vmem = pl.BlockSpec(memory_space=pltpu.VMEM)
    dma = pltpu.SemaphoreType.DMA
    return pl.pallas_call(
        functools.partial(body, (nf, nt)),
        out_shape=jax.ShapeDtypeStruct((rows, fd), BF16),
        in_specs=[hbm, vmem, hbm, hbm, vmem, vmem, vmem, hbm, vmem, hbm, hbm, vmem, vmem, hbm, vmem],
        out_specs=vmem,
        scratch_shapes=[
            pltpu.VMEM((nf, 2 * kz + 2 * kb, LANE), BF16),
            pltpu.VMEM((nf, kz, 2 * ffd), BF16),
            pltpu.VMEM((nf, ffd, mlp_down.shape[1]), BF16),
            pltpu.VMEM((rows, dm), BF16),
            pltpu.VMEM((rows, ca), BF16),
            pltpu.VMEM((rows, dm), BF16),
            pltpu.VMEM((rows, dm), BF16),
            pltpu.VMEM((rows + 2 * PAD, fc), F32),
            pltpu.VMEM((rows + 2 * PAD, 2 * ffd), F32),
            pltpu.VMEM((rows, ca), BF16),
            pltpu.VMEM((rows, ffd), BF16),
            pltpu.VMEM((RCHUNKS, nx, hr, fd), F32),
            pltpu.VMEM((RCHUNKS, nx, hr, fd), BF16),
            pltpu.VMEM((RCHUNKS, nx, hr, fd), BF16),
            pltpu.VMEM((RCHUNKS, hr, fd), BF16),
            pltpu.VMEM((RCHUNKS, hr, fd), BF16),
            pltpu.VMEM((RCHUNKS, 2, hr, fd), BF16),
            pltpu.VMEM((RCHUNKS, 2, hr, fd), BF16),
            pltpu.VMEM((rows, fd), F32),
            pltpu.VMEM((RCHUNKS, 8, hr), F32),
            pltpu.VMEM((RCHUNKS, nt - 1, 8, hr), F32),
            pltpu.VMEM((ffd, kz), BF16),
            pltpu.VMEM((ffd, kz), BF16),
            pltpu.VMEM((8, 2 * ffd), F32),
            dma((8,)),
            dma((10,)),
            dma((10, half + 1, 2)),
            dma((4,)),
            dma((4, 2)),
            dma((3,)),
            dma((3, CHUNKS, 5)),
            dma((3,)),
            dma((RCHUNKS, 4)),
            dma((1,)),
            dma((RCHUNKS,)),
        ],
        compiler_params=pltpu.CompilerParams(
            collective_id=0, has_side_effects=True, vmem_limit_bytes=67043328
        ),
        name="layer",
    )(
        tokens,
        row(mix_gain),
        value_proj,
        gate_proj,
        conv_taps,
        row(chan_gain),
        row(chan_shift),
        mix_out,
        row(mlp_gain),
        mlp_gate.T,
        mlp_up.T,
        gate_taps,
        up_taps,
        mlp_down,
        row(final_gain),
    )


def solution(mesh):
    return jax.shard_map(
        functools.partial(local, mesh),
        mesh=mesh,
        in_specs=(
            P(("grp", "fs"), "tp"),
            P(),
            P("fs", "tp"),
            P("fs", "tp"),
            P(None, "tp"),
            P(),
            P(),
            P("fs", "tp"),
            P(),
            P("fs", "tp"),
            P("fs", "tp"),
            P(None, "tp"),
            P(None, "tp"),
            P("tp", "fs"),
            P("tp"),
        ),
        out_specs=P(("grp", "fs"), "tp"),
        check_vma=False,
    )
```

time: 169 us -> 151 us (0.89)
  Pallas kernels: 161 us -> 148 us
  local copies, waits for them, and re-layouts: 7.93 us -> 1.87 us
    pallas_call x1, Pallas kernels: 161 us -> 148 us  [local(): pl.pallas_call(functools.partial(body, (nf, nt)), out_shape=jax.ShapeDtyp...]
    slice x16 -> x0, local copies, waits for them, and re-layouts: 3.99 us -> none  [the longest x4 1.6 us: side(): b[:, :cut]]
where the time goes in v2:
time: 151 us; the launch traced here: 150 us
  Pallas kernels  148 us (98%)
  local copies, waits for them, and re-layouts  1.87 us (1%)
    pallas_call x1, Pallas kernels, local(): pl.pallas_call(functools.partial(body, (nf, nt)), out_shape=jax.ShapeDtyp...  148 us

profile of v2, /device:TPU:33, one launch (start us, length us, event | category | flops | bytes accessed | tf_op | source)
XLA Modules:
  0.0 150.4 jit_solution(8173471876945862070)
XLA Ops:
  0.0 148.5 %layer.1 = bf16[1024,256]{1,0:T(8,128)(2,1)} custom-call(bf16[1024,256]{1,0:T(8,128)(2,1)} %tokens.1, f32[1,2048]{1,0:T(1,128)} %bitcast.9, bf16[128,128]{1,0:T(8,128)(2,1)} %value_own.1, bf16[128,128]{1,0:T(8,128)(2,1)} %gate_own.1, f32[31,128]{1,0:T(8,128)} %conv_taps.1, f32[1,1024]{1,0:T(1,128)} %bitcast.11, f32[1,1024]{1,0:T(1,128)} %bitcast.12, ...), custom_call_target="tpu_custom_call" | custom-call | tf_op jit(solution)/shard_map/layer/pallas_call | solution.py:625
  148.5 1.9 %copy.17 = bf16[1024,256]{1,0:T(8,128)(2,1)} copy(bf16[1024,256]{1,0:T(8,128)(2,1)} %layer.1) | data formatting | bytes 1048576

commit v3 on v2

--- a/solution.py
+++ b/solution.py
@@ -14,7 +14,7 @@
 LANE = 128
 PAD = 16
 EACH = 3
-VAL, GAT, OUT, CP0, CX, CP1, CA, CB, DA, DB = range(10)
+VAL, GAT, OUT, CP0, CP1, CP2, CA, CB, DN = range(9)
 TOK, CONV, MIX = range(3)
 
 
@@ -127,6 +127,11 @@
     def left_here(ref, sem):
         remote(ref, ref, sem, sem, partner).wait_send()
 
+    barrier = pltpu.get_barrier_semaphore()
+    peers = [dev_tp(lax.rem(tp + o, nt)) for o in range(1, nt)] + [zdev[0], zdev[1], peer_y]
+    for dev in peers:
+        pl.semaphore_signal(barrier, inc=1, device_id=dev, device_id_type=pl.DeviceIdType.MESH)
+
     def own_c(r0, n):
         return wc.at[fs, pl.ds(r0, n)]
 
@@ -145,11 +150,6 @@
     for copy in local:
         copy.start()
 
-    barrier = pltpu.get_barrier_semaphore()
-    peers = [dev_tp(lax.rem(tp + o, nt)) for o in range(1, nt)] + [zdev[0], zdev[1], peer_y]
-    for dev in peers:
-        pl.semaphore_signal(barrier, inc=1, device_id=dev, device_id_type=pl.DeviceIdType.MESH)
-
     whole = full_tiles // LANE
     cut = EACH * LANE
     at = 0
@@ -178,7 +178,7 @@
 
     for i in (5, 6):
         local[i].wait()
-    soon = (0, EACH, 2 * EACH)
+    soon = (0, 1, EACH, EACH + 1)
     for pos in soon:
         pack(pos)
 
@@ -197,20 +197,19 @@
         GAT: (wab, (kz, kz), None),
         OUT: (wab, (2 * kz, 2 * kb), None),
         CP0: (wc, None, (0, 1)),
-        CX: (wc, None, (2 * EACH, 1)),
-        CP1: (wc, None, (1, EACH - 1)),
-        CA: (wc, None, (2 * EACH + 1, 2)),
-        CB: (wc, None, (2 * EACH + 3, 2)),
-        DA: (wd, (0, dhalf // 2), None),
-        DB: (wd, (dhalf // 2, dhalf // 2), None),
+        CP1: (wc, None, (1, 1)),
+        CP2: (wc, None, (2, EACH - 2)),
+        CA: (wc, None, (2 * EACH, 2)),
+        CB: (wc, None, (2 * EACH + 2, 3)),
+        DN: (wd, (0, dhalf), None),
     }
-    ylane = {CP0: 0, CP1: 1, DA: 2, DB: 3}
+    ylane = {CP0: 0, CP1: 1, CP2: 2, DN: 3}
 
     def zslice(lane, idx, h=None, who=None):
         who = par if who is None else who
         ref, span, cols = lanes[lane]
         r0, n = (0, ref.shape[1]) if span is None else span
-        if lane in (DA, DB):
+        if lane == DN:
             r0 = pl.multiple_of(who * dhalf + r0, 16)
         if h is not None:
             r0, n = r0 + h * (n // 2), n // 2
@@ -219,7 +218,7 @@
         if cols is None:
             return ref.at[idx, pl.ds(r0, n)]
         c0 = cols[0] * LANE
-        if lane in (CP0, CP1):
+        if lane in (CP0, CP1, CP2):
             c0 = pl.multiple_of(who * (EACH * LANE) + c0, LANE)
         return ref.at[idx, pl.ds(r0, n), pl.ds(c0, cols[1] * LANE)]
 
@@ -230,16 +229,16 @@
 
     def z_own(lane):
         for d in range(2):
-            send(zslice(lane, fs), zs.at[lane], zr.at[lane, 1, d], zdev[d])
+            send(zslice(lane, fs), zs.at[lane], zr.at[lane, 0, d], zdev[d])
 
     def z_visit(lane, s):
         h = [None, None] if s < half else [0, 1]
         for d in range(2):
             idx = zidx(s, d)
-            landed(zslice(lane, idx, h[d]), zr.at[lane, s, d])
+            landed(zslice(lane, idx, h[d]), zr.at[lane, s - 1, d])
             if s < half:
                 piece = zslice(lane, idx, d if s == half - 1 else None)
-                send(piece, zs.at[lane], zr.at[lane, s + 1, d], zdev[d])
+                send(piece, zs.at[lane], zr.at[lane, s, d], zdev[d])
         if lane in ylane:
             y, part = ylane[lane], 0 if s <= near else 1
             for d in range(2):
@@ -249,7 +248,7 @@
         count = 2 * near if part == 0 else nf - 1 - 2 * near
         landed(zslice(lane, pl.ds(0, count), None, other), yr.at[ylane[lane], part])
 
-    phases = ((VAL, GAT, OUT, CP0, CX), (CP1, CA, CB, DA, DB))
+    phases = ((VAL, GAT, OUT, CP0, CP1), (CP2, DN, CA, CB))
     queue = [(lane, s) for group in phases for s in range(1, half + 1) for lane in group]
 
     def pump(n):
@@ -518,7 +517,7 @@
     norm(tf, mix_gain, 3)
     pump_to(GAT, half)
     mat_a(0)
-    pump_to(CX, half)
+    pump_to(CP1, half)
     for r in range(1, CHUNKS):
         mat_a(r)
         conv(r - 1)
@@ -529,7 +528,6 @@
     ag_v1(CONV, 0)
     pump(1)
     ag_v1(CONV, 1)
-    pump(1)
     ag_v1(CONV, 2)
     pump(1)
     ag_v1(CONV, 3)
@@ -541,7 +539,8 @@
         ag_done(CONV, r)
         mix(r)
         ag_own(MIX, r)
-        pump(1)
+        if r != 1:
+            pump(1)
         if r + 2 < CHUNKS:
             ag_v2(CONV, r + 2)
     pump(1)
@@ -557,27 +556,30 @@
         norm(mf, mlp_gain, r)
         pump(1)
     pump_to(CB, near)
-    y_done(CP0, 0)
-    y_done(CP1, 0)
+    for lane in (CP0, CP1, CP2):
+        y_done(lane, 0)
     for r in range(CHUNKS):
         mat_c(r)
         pump(2)
     pump(len(queue))
-    y_done(CP0, 1)
-    y_done(CP1, 1)
-    stages = {2: hidden, 3: rs_a, 4: rs_b, 6: rs_c, 8: rs_d, 10: rs_e}
+    for lane in (CP0, CP1, CP2):
+        y_done(lane, 1)
+    stages = {1: rs_b, 3: rs_c, 7: rs_d, 10: rs_e}
     per = cr // hr
     for tick in range(RCHUNKS + max(stages)):
-        if tick % per == 0 and tick // per < CHUNKS:
-            mat_late(tick // per)
-        for lag in sorted(stages, reverse=True):
-            r = tick - lag
-            if 0 <= r < RCHUNKS:
-                if lag == 3 and r == 0:
-                    for lane in (DA, DB):
-                        y_done(lane, 0)
-                        y_done(lane, 1)
-                stages[lag](r)
+        for lag, stage in stages.items():
+            if 0 <= tick - lag < RCHUNKS:
+                stage(tick - lag)
+        if tick < RCHUNKS:
+            if tick == 0:
+                mat_late(0)
+            if tick % per == per - 1 and tick // per + 1 < CHUNKS:
+                mat_late(tick // per + 1)
+            hidden(tick)
+            if tick == 0:
+                y_done(DN, 0)
+                y_done(DN, 1)
+            rs_a(tick)
 
     for lane in lanes:
         left_here(zslice(lane, pl.ds(0, nf - 1)), zs.at[lane])
@@ -653,8 +655,8 @@
             pltpu.VMEM((ffd, kz), BF16),
             pltpu.VMEM((8, 2 * ffd), F32),
             dma((8,)),
-            dma((10,)),
-            dma((10, half + 1, 2)),
+            dma((9,)),
+            dma((9, half, 2)),
             dma((4,)),
             dma((4, 2)),
             dma((3,)),

time: 151 us -> 145 us (0.960)
  Pallas kernels: 148 us -> 143 us
    pallas_call x1, Pallas kernels: 148 us -> 143 us  [local(): pl.pallas_call(functools.partial(body, (nf, nt)), out_shape=jax.ShapeDtyp...]
where the time goes in v3:
time: 145 us
  Pallas kernels  143 us (99%)
  local copies, waits for them, and re-layouts  1.87 us (1%)
    pallas_call x1, Pallas kernels, local(): pl.pallas_call(functools.partial(body, (nf, nt)), out_shape=jax.ShapeDtyp...  143 us

profile of v3, /device:TPU:33, one launch (start us, length us, event | category | flops | bytes accessed | tf_op | source)
XLA Modules:
  0.0 144.8 jit_solution(9944193604868152260)
XLA Ops:
  0.0 142.9 %layer.1 = bf16[1024,256]{1,0:T(8,128)(2,1)} custom-call(bf16[1024,256]{1,0:T(8,128)(2,1)} %tokens.1, f32[1,2048]{1,0:T(1,128)} %bitcast.9, bf16[128,128]{1,0:T(8,128)(2,1)} %value_own.1, bf16[128,128]{1,0:T(8,128)(2,1)} %gate_own.1, f32[31,128]{1,0:T(8,128)} %conv_taps.1, f32[1,1024]{1,0:T(1,128)} %bitcast.11, f32[1,1024]{1,0:T(1,128)} %bitcast.12, ...), custom_call_target="tpu_custom_call" | custom-call | tf_op jit(solution)/shard_map/layer/pallas_call | solution.py:627
  143.0 1.9 %copy.17 = bf16[1024,256]{1,0:T(8,128)(2,1)} copy(bf16[1024,256]{1,0:T(8,128)(2,1)} %layer.1) | data formatting | bytes 1048576

commit v4 on v3

--- a/solution.py
+++ b/solution.py
@@ -14,7 +14,7 @@
 LANE = 128
 PAD = 16
 EACH = 3
-VAL, GAT, OUT, CP0, CP1, CP2, CA, CB, DN = range(9)
+VAL, GAT, OUT, CP0, CP1, CP2, CS, CA, CB, DN = range(10)
 TOK, CONV, MIX = range(3)
 
 
@@ -199,18 +199,19 @@
         CP0: (wc, None, (0, 1)),
         CP1: (wc, None, (1, 1)),
         CP2: (wc, None, (2, EACH - 2)),
-        CA: (wc, None, (2 * EACH, 2)),
-        CB: (wc, None, (2 * EACH + 2, 3)),
+        CS: (wc, (0, kz // 2), (2 * EACH, 1)),
+        CA: (wc, None, (2 * EACH + 1, 2)),
+        CB: (wc, None, (2 * EACH + 3, 2)),
         DN: (wd, (0, dhalf), None),
     }
-    ylane = {CP0: 0, CP1: 1, CP2: 2, DN: 3}
+    ylane = {CP0: 0, CP1: 1, CP2: 2, CS: 3, DN: 4}
 
     def zslice(lane, idx, h=None, who=None):
         who = par if who is None else who
         ref, span, cols = lanes[lane]
         r0, n = (0, ref.shape[1]) if span is None else span
-        if lane == DN:
-            r0 = pl.multiple_of(who * dhalf + r0, 16)
+        if lane in (DN, CS):
+            r0 = pl.multiple_of(who * n, 16)
         if h is not None:
             r0, n = r0 + h * (n // 2), n // 2
         if not isinstance(r0, int):
@@ -248,7 +249,7 @@
         count = 2 * near if part == 0 else nf - 1 - 2 * near
         landed(zslice(lane, pl.ds(0, count), None, other), yr.at[ylane[lane], part])
 
-    phases = ((VAL, GAT, OUT, CP0, CP1), (CP2, DN, CA, CB))
+    phases = ((VAL, GAT, OUT, CP0, CP1), (CP2, DN, CS, CA, CB))
     queue = [(lane, s) for group in phases for s in range(1, half + 1) for lane in group]
 
     def pump(n):
@@ -525,13 +526,10 @@
         pump(1)
     conv(CHUNKS - 1)
     ag_own(CONV, CHUNKS - 1)
-    ag_v1(CONV, 0)
     pump(1)
-    ag_v1(CONV, 1)
-    ag_v1(CONV, 2)
-    pump(1)
-    ag_v1(CONV, 3)
-    pump(1)
+    for r in range(CHUNKS):
+        ag_v1(CONV, r)
+        pump(1)
     ag_v2(CONV, 0)
     ag_v2(CONV, 1)
     pump(1)
@@ -539,47 +537,55 @@
         ag_done(CONV, r)
         mix(r)
         ag_own(MIX, r)
-        if r != 1:
-            pump(1)
+        pump(1)
         if r + 2 < CHUNKS:
             ag_v2(CONV, r + 2)
-    pump(1)
     for r in range(CHUNKS):
-        pump(2)
+        pump(2 if r != CHUNKS - 1 else 3)
         ag_v1(MIX, r)
-    pump(1)
     for r in range(CHUNKS):
         ag_v2(MIX, r)
-        pump(1)
+        pump(2 if r < 2 else 1)
     for r in range(CHUNKS):
         ag_done(MIX, r)
         norm(mf, mlp_gain, r)
         pump(1)
     pump_to(CB, near)
-    for lane in (CP0, CP1, CP2):
+    for lane in (CP0, CP1, CP2, CS):
         y_done(lane, 0)
     for r in range(CHUNKS):
         mat_c(r)
-        pump(2)
+        pump(1)
     pump(len(queue))
-    for lane in (CP0, CP1, CP2):
+    for lane in (CP0, CP1, CP2, CS):
         y_done(lane, 1)
-    stages = {1: rs_b, 3: rs_c, 7: rs_d, 10: rs_e}
     per = cr // hr
-    for tick in range(RCHUNKS + max(stages)):
-        for lag, stage in stages.items():
-            if 0 <= tick - lag < RCHUNKS:
-                stage(tick - lag)
+
+    def if_chunk(stage, r):
+        if 0 <= r < RCHUNKS:
+            stage(r)
+
+    for tick in range(RCHUNKS + 10):
+        late = False
         if tick < RCHUNKS:
             if tick == 0:
                 mat_late(0)
             if tick % per == per - 1 and tick // per + 1 < CHUNKS:
                 mat_late(tick // per + 1)
+                late = True
             hidden(tick)
             if tick == 0:
                 y_done(DN, 0)
                 y_done(DN, 1)
+        if_chunk(rs_c, tick - 3)
+        if late or tick >= RCHUNKS:
+            if_chunk(rs_b, tick - 1)
+        if tick < RCHUNKS:
             rs_a(tick)
+            if not late:
+                if_chunk(rs_b, tick - 1)
+        if_chunk(rs_d, tick - 7)
+        if_chunk(rs_e, tick - 10)
 
     for lane in lanes:
         left_here(zslice(lane, pl.ds(0, nf - 1)), zs.at[lane])
@@ -655,10 +661,10 @@
             pltpu.VMEM((ffd, kz), BF16),
             pltpu.VMEM((8, 2 * ffd), F32),
             dma((8,)),
-            dma((9,)),
-            dma((9, half, 2)),
-            dma((4,)),
-            dma((4, 2)),
+            dma((10,)),
+            dma((10, half, 2)),
+            dma((5,)),
+            dma((5, 2)),
             dma((3,)),
             dma((3, CHUNKS, 5)),
             dma((3,)),

time: 145 us -> 145 us (level)
  no operation moved by 1% of the time
where the time goes in v4:
time: 145 us; the launch traced here: 144 us
  Pallas kernels  143 us (99%)
  local copies, waits for them, and re-layouts  1.87 us (1%)
    pallas_call x1, Pallas kernels, local(): pl.pallas_call(functools.partial(body, (nf, nt)), out_shape=jax.ShapeDtyp...  143 us

profile of v4, /device:TPU:33, one launch (start us, length us, event | category | flops | bytes accessed | tf_op | source)
XLA Modules:
  0.0 144.4 jit_solution(14901938030911201654)
XLA Ops:
  0.0 142.6 %layer.1 = bf16[1024,256]{1,0:T(8,128)(2,1)} custom-call(bf16[1024,256]{1,0:T(8,128)(2,1)} %tokens.1, f32[1,2048]{1,0:T(1,128)} %bitcast.9, bf16[128,128]{1,0:T(8,128)(2,1)} %value_own.1, bf16[128,128]{1,0:T(8,128)(2,1)} %gate_own.1, f32[31,128]{1,0:T(8,128)} %conv_taps.1, f32[1,1024]{1,0:T(1,128)} %bitcast.11, f32[1,1024]{1,0:T(1,128)} %bitcast.12, ...), custom_call_target="tpu_custom_call" | custom-call | tf_op jit(solution)/shard_map/layer/pallas_call | solution.py:633
  142.6 1.9 %copy.17 = bf16[1024,256]{1,0:T(8,128)(2,1)} copy(bf16[1024,256]{1,0:T(8,128)(2,1)} %layer.1) | data formatting | bytes 1048576

commit v5 on v4

--- a/solution.py
+++ b/solution.py
@@ -249,7 +249,7 @@
         count = 2 * near if part == 0 else nf - 1 - 2 * near
         landed(zslice(lane, pl.ds(0, count), None, other), yr.at[ylane[lane], part])
 
-    phases = ((VAL, GAT, OUT, CP0, CP1), (CP2, DN, CS, CA, CB))
+    phases = ((VAL, GAT, OUT, CP0, CP1), (CP2, CS, DN, CA, CB))
     queue = [(lane, s) for group in phases for s in range(1, half + 1) for lane in group]
 
     def pump(n):
@@ -577,13 +577,13 @@
             if tick == 0:
                 y_done(DN, 0)
                 y_done(DN, 1)
-        if_chunk(rs_c, tick - 3)
         if late or tick >= RCHUNKS:
             if_chunk(rs_b, tick - 1)
         if tick < RCHUNKS:
             rs_a(tick)
             if not late:
                 if_chunk(rs_b, tick - 1)
+        if_chunk(rs_c, tick - 3)
         if_chunk(rs_d, tick - 7)
         if_chunk(rs_e, tick - 10)
 

time: 145 us -> 142 us (0.979)
  Pallas kernels: 143 us -> 140 us
    pallas_call x1, Pallas kernels: 143 us -> 140 us  [local(): pl.pallas_call(functools.partial(body, (nf, nt)), out_shape=jax.ShapeDtyp...]
where the time goes in v5:
time: 142 us
  Pallas kernels  140 us (99%)
  local copies, waits for them, and re-layouts  1.87 us (1%)
    pallas_call x1, Pallas kernels, local(): pl.pallas_call(functools.partial(body, (nf, nt)), out_shape=jax.ShapeDtyp...  140 us

profile of v5, /device:TPU:33, one launch (start us, length us, event | category | flops | bytes accessed | tf_op | source)
XLA Modules:
  0.0 141.7 jit_solution(10071519061924161995)
XLA Ops:
  0.0 139.8 %layer.1 = bf16[1024,256]{1,0:T(8,128)(2,1)} custom-call(bf16[1024,256]{1,0:T(8,128)(2,1)} %tokens.1, f32[1,2048]{1,0:T(1,128)} %bitcast.9, bf16[128,128]{1,0:T(8,128)(2,1)} %value_own.1, bf16[128,128]{1,0:T(8,128)(2,1)} %gate_own.1, f32[31,128]{1,0:T(8,128)} %conv_taps.1, f32[1,1024]{1,0:T(1,128)} %bitcast.11, f32[1,1024]{1,0:T(1,128)} %bitcast.12, ...), custom_call_target="tpu_custom_call" | custom-call | tf_op jit(solution)/shard_map/layer/pallas_call | solution.py:633
  139.8 1.9 %copy.17 = bf16[1024,256]{1,0:T(8,128)(2,1)} copy(bf16[1024,256]{1,0:T(8,128)(2,1)} %layer.1) | data formatting | bytes 1048576
